TPU v7x, 32 devices: a whole 2x2x4 slice. The times are simulated.
32 devices in a mesh: gr: 2 (over x), fs: 8 (over z, y), tp: 2 (over core).
Axes of the slice: x: 2, y: 2, z: 4, core: 2. Of those that a mesh axis runs over, the one named last changes fastest.
Arguments:
- prompt_tokens: bfloat16 [4608, 2048], P(('gr', 'fs', 'tp')), may hold values from -6 to 6
- up_master: float32 [2048, 8192], P(('gr', 'fs'), 'tp'), may hold values from -0.125 to 0.125
- down_master: float32 [2048, 8192], P(('gr', 'fs'), 'tp'), may hold values from -0.0625 to 0.0625
- norm_gain: float32 [2048], P(('gr', 'fs')), may hold values from 0.1 to 1.9
Outputs:
- sampler_up: bfloat16 [2048, 8192], P(None, ('gr', 'tp'))
- sampler_down: bfloat16 [2048, 8192], P(None, ('gr', 'tp'))
- prompt_out: bfloat16 [4608, 2048], P(('gr', 'fs', 'tp'))
All inputs are finite; a program needn't handle non-finite values.
Results may differ from a plain program's by a relative error of at most 0.009.
Values may be sent and summed in bfloat16 or wider, within the bound.
No kernel may reach another device: no remote copies, remote signals or barrier semaphores. Data moves between devices by JAX's collectives and lax.ppermute only.
A program may use at most 128 MiB of HBM per device.

v0:
```python
import jax
import jax.numpy as jnp
from jax import lax
from jax.sharding import PartitionSpec as P


def regroup(matrix, groups, shards):
    block = matrix.shape[0] // (groups * shards)
    shaped = matrix.reshape(shards, groups, block, matrix.shape[1])
    return shaped.transpose(1, 0, 2, 3).reshape(groups * shards * block, matrix.shape[1])


def body(prompt_tokens, up_master, down_master, norm_gain):
    up_local = (norm_gain[:, None] * up_master).astype(jnp.bfloat16)
    down_local = down_master.astype(jnp.bfloat16)
    moved = (
        lax.all_to_all(
            lax.all_to_all(up_local, "tp", split_axis=1, concat_axis=0, tiled=True),
            "gr",
            split_axis=0,
            concat_axis=0,
            tiled=True,
        ),
        lax.all_to_all(
            lax.all_to_all(down_local, "tp", split_axis=1, concat_axis=0, tiled=True),
            "gr",
            split_axis=0,
            concat_axis=0,
            tiled=True,
        ),
    )
    stacked = (
        lax.all_gather(moved[0], "fs", axis=0, tiled=True),
        lax.all_gather(moved[1], "fs", axis=0, tiled=True),
    )
    groups = lax.axis_size("gr")
    shards = lax.axis_size("fs")
    sampler_up = regroup(stacked[0], groups, shards)
    sampler_down = regroup(stacked[1], groups, shards)
    values = prompt_tokens.astype(jnp.float32)
    center = jnp.mean(values, axis=-1, keepdims=True)
    variance = jnp.mean(jnp.square(values - center), axis=-1, keepdims=True)
    normed = ((values - center) * lax.rsqrt(variance + 1e-05)).astype(jnp.bfloat16)
    lifted = jax.nn.relu(
        jnp.dot(
            lax.all_gather(normed, ("gr", "tp"), axis=0, tiled=True),
            sampler_up,
            preferred_element_type=jnp.float32,
        )
    )
    hidden = (lifted * lifted).astype(jnp.bfloat16)
    partial_value = lax.dot_general(
        hidden, sampler_down, (((1,), (1,)), ((), ())), preferred_element_type=jnp.float32
    )
    summed = lax.psum_scatter(
        lax.optimization_barrier(partial_value.astype(jnp.bfloat16))
        .astype(jnp.float32)
        .astype(jnp.bfloat16),
        ("gr", "tp"),
        scatter_dimension=0,
        tiled=True,
    )
    return (sampler_up, sampler_down, summed)


def solution(mesh):
    placed = (
        P(("gr", "fs", "tp"), None),
        P(("gr", "fs"), "tp"),
        P(("gr", "fs"), "tp"),
        P(("gr", "fs")),
    )
    return jax.shard_map(
        body,
        mesh=mesh,
        in_specs=placed,
        out_specs=(P(None, ("gr", "tp")), P(None, ("gr", "tp")), P(("gr", "fs", "tp"), None)),
        check_vma=False,
    )
```

profile of v0, /device:TPU:0, one launch (start us, length us, event | category | flops | bytes accessed | tf_op | source)
XLA Modules:
  0.0 364.8 jit_solution(9255359435102102182)
XLA Ops:
  7.2 0.0 copy-start.2
  7.2 0.0 all-gather.4.cloned.1.call-start
  7.2 1.9 copy.7
  9.1 0.0 copy-done.2
  9.2 0.1 multiply_convert_fusion.1
  9.3 4.6 %all_to_all.50 = bf16[128,2,2048]{0,2,1:T(8,128)(2,1)S(1)} all-to-all(bf16[128,2,2048]{0,2,1:T(8,128)(2,1)S(1)} %bitcast.35), channel_id=1, replica_groups=mesh['gr'=2,'fs'=8,'tp'=2] {'tp'}, dimensions={1} | all-to-all | bytes 2097152 | tf_op jit(solution)/shard_map/all_to_all | solution.py:18
  13.8 0.0 copy-start.1
  13.8 18.0 %all_to_all.51 = bf16[2,128,2048]{1,2,0:T(8,128)(2,1)S(1)} all-to-all(bf16[2,128,2048]{1,2,0:T(8,128)(2,1)S(1)} %bitcast.36), channel_id=1, replica_groups=mesh['gr'=2,'fs'=8,'tp'=2] {'gr'}, dimensions={0} | all-to-all | bytes 2097152 | tf_op jit(solution)/shard_map/all_to_all | solution.py:17
  31.9 1.3 copy.8
  33.2 0.0 all-gather.4.cloned.1.call-update
  33.2 0.0 all-gather.6.cloned.1.call-start
  33.3 0.0 copy-done.1
  33.3 0.7 copy.10
  34.0 4.6 %all_to_all.52 = bf16[128,2,2048]{0,2,1:T(8,128)(2,1)S(1)} all-to-all(bf16[128,2,2048]{0,2,1:T(8,128)(2,1)S(1)} %bitcast.32), channel_id=1, replica_groups=mesh['gr'=2,'fs'=8,'tp'=2] {'tp'}, dimensions={1} | all-to-all | bytes 2097152 | tf_op jit(solution)/shard_map/all_to_all | solution.py:25
  38.6 0.0 copy-start
  38.6 16.7 %all_to_all.53 = bf16[2,128,2048]{1,2,0:T(8,128)(2,1)S(1)} all-to-all(bf16[2,128,2048]{1,2,0:T(8,128)(2,1)S(1)} %bitcast.37), channel_id=1, replica_groups=mesh['gr'=2,'fs'=8,'tp'=2] {'gr'}, dimensions={0} | all-to-all | bytes 2097152 | tf_op jit(solution)/shard_map/all_to_all | solution.py:24
  55.4 1.3 copy.11
  56.7 0.0 all-gather.6.cloned.1.call-update
  56.7 0.0 all-gather.8.cloned.1.call-start
  56.7 0.0 copy-done
  56.7 0.2 convert_reduce_fusion
  56.9 0.3 fusion.2
  57.2 1.2 fusion.3
  58.4 0.0 all-gather.8.cloned.1.call-update
  58.4 0.0 reduce-scatter.2.cloned.1.call-start
  58.5 99.9 %all-gather.4.cloned.1.call-done = bf16[2048,2048]{1,0:T(8,128)(2,1)} async-done(((bf16[256,2048]{1,0:T(8,128)(2,1)}), bf16[2048,2048]{1,0:T(8,128)(2,1)}) %all-gather.4.cloned.1.call-update) | async-done | bytes 8388624 | tf_op jit(solution)/shard_map/all_gather | solution.py:33
  158.4 8.4 %copy.9 = bf16[2,8,128,2048]{3,2,1,0:T(8,128)(2,1)} copy(bf16[2,8,128,2048]{3,2,0,1:T(8,128)(2,1)} %bitcast.26) | data formatting | bytes 16777216 | tf_op jit(solution)/shard_map/transpose | solution.py:10
  166.8 116.4 %all-gather.6.cloned.1.call-done = bf16[2048,2048]{1,0:T(8,128)(2,1)} async-done(((bf16[256,2048]{1,0:T(8,128)(2,1)}), bf16[2048,2048]{1,0:T(8,128)(2,1)}) %all-gather.6.cloned.1.call-update) | async-done | bytes 8388624 | tf_op jit(solution)/shard_map/all_gather | solution.py:34
  283.2 8.6 %copy.12 = bf16[2,8,128,2048]{3,2,1,0:T(8,128)(2,1)} copy(bf16[2,8,128,2048]{3,2,0,1:T(8,128)(2,1)} %bitcast.27) | data formatting | bytes 16777216 | tf_op jit(solution)/shard_map/transpose | solution.py:10
  291.8 15.8 %all-gather.8.cloned.1.call-done = bf16[576,2048]{1,0:T(8,128)(2,1)} async-done(((bf16[144,2048]{1,0:T(8,128)(2,1)}), bf16[576,2048]{1,0:T(8,128)(2,1)}) %all-gather.8.cloned.1.call-update) | async-done | bytes 2359312 | tf_op jit(solution)/shard_map/all_gather | solution.py:46
  307.6 17.7 %convolution_convert_fusion = bf16[576,2048]{1,0:T(8,128)(2,1)} fusion(bf16[2048,2048]{1,0:T(8,128)(2,1)} %bitcast.30, bf16[576,2048]{1,0:T(8,128)(2,1)} %all-gather.8.cloned.1.call-done, bf16[2048,2048]{1,0:T(8,128)(2,1)} %bitcast.28), kind=kOutput, calls=%fused_computation.1 | convolution fusion | flops 9668395008 | bytes 21495808 | tf_op jit(solution)/shard_map/dot_general | solution.py:52
  325.3 0.0 reduce-scatter.2.cloned.1.call-update
  325.3 33.0 %reduce-scatter.2.cloned.1.call-done = bf16[144,2048]{1,0:T(8,128)(2,1)} async-done(((bf16[576,2048]{1,0:T(8,128)(2,1)}), bf16[144,2048]{1,0:T(8,128)(2,1)}) %reduce-scatter.2.cloned.1.call-update) | async-done | bytes 589840 | tf_op jit(solution)/shard_map/reduce_scatter | solution.py:55
  (2 shorter events, 0.0 us)
Async XLA Ops:
  7.2 2.0 copy-start.2
  7.2 151.2 %all-gather.4.cloned.1.call-start = ((), (), s32[]{:S(2)}) async-start(), calls=%async_computation.5 | async-start | bytes 9437184 | tf_op jit(solution)/shard_map/all_gather | solution.py:33
  13.8 19.4 %copy-start.1 = (f32[128,4096]{1,0:T(8,128)S(1)}, f32[128,4096]{1,0:T(8,128)}, u32[]{:S(2)}) copy-start(f32[128,4096]{1,0:T(8,128)} %param.6) | copy-start | bytes 6291460
  33.2 249.9 %all-gather.6.cloned.1.call-start = ((), (), s32[]{:S(2)}) async-start(), calls=%async_computation.6 | async-start | bytes 9437184 | tf_op jit(solution)/shard_map/all_gather | solution.py:34
  38.6 18.1 %copy-start = (bf16[144,2048]{1,0:T(8,128)(2,1)S(1)}, bf16[144,2048]{1,0:T(8,128)(2,1)}, u32[]{:S(2)}) copy-start(bf16[144,2048]{1,0:T(8,128)(2,1)} %param.4) | copy-start | bytes 1769476
  56.7 250.9 %all-gather.8.cloned.1.call-start = ((), (), s32[]{:S(2)}) async-start(), calls=%async_computation.7 | async-start | bytes 2949120 | tf_op jit(solution)/shard_map/all_gather | solution.py:46
  58.4 299.9 %reduce-scatter.2.cloned.1.call-start = ((), (), s32[]{:S(2)}) async-start(), calls=%async_computation.8 | async-start | bytes 2949120 | tf_op jit(solution)/shard_map/reduce_scatter | solution.py:55
Sparse Core Ops, SparseCore 0:
  33.3 124.9 all-gather.3
  160.5 122.6 all-gather.5
  285.3 22.2 all-gather.7
  325.5 32.8 reduce-scatter.1
where the time goes:
time: 365 us
  waiting for transfers between devices  265 us (73%)
  blocking collectives  43.9 us (12%)
  local copies, waits for them, and re-layouts  22.3 us (6%)
  matrix products  17.7 us (5%)
  between operations  13.8 us (4%)
    all_gather x1, waiting for transfers between devices, body(): lax.all_gather(moved[1], 'fs', axis=0, tiled=True)  116 us
    all_gather x1, waiting for transfers between devices, body(): lax.all_gather(moved[0], 'fs', axis=0, tiled=True)  99.9 us
    reduce_scatter x1, waiting for transfers between devices, body(): lax.psum_scatter(lax.optimization_barrier(partial_value.astype(jnp.bfloat...  33 us
    all_to_all x1, blocking collectives, body(): lax.all_to_all(lax.all_to_all(up_local, 'tp', split_axis=1, concat_axis=0...  18 us
    dot_general x1, matrix products, body(): lax.dot_general(hidden, sampler_down, (((1,), (1,)), ((), ())), preferred...  17.7 us
    transpose x2, local copies, waits for them, and re-layouts, regroup(): shaped.transpose(1, 0, 2, 3)  17.1 us
    all_to_all x1, blocking collectives, body(): lax.all_to_all(lax.all_to_all(down_local, 'tp', split_axis=1, concat_axis...  16.7 us
    all_gather x1, waiting for transfers between devices, body(): lax.all_gather(normed, ('gr', 'tp'), axis=0, tiled=True)  15.8 us
  transfers between devices with their start and end apart: 4, of which 4 were waited for; matrix products, arithmetic and copies ran while one was open for 6% of the time, Pallas kernels for 0%

commit v1 on v0

v1 whole, which is shorter than its diff:
```python
import jax
import jax.numpy as jnp
from jax import lax
from jax.sharding import PartitionSpec as P


PAIR = 2
GROUP = ("gr", "tp")


def line_pairs(links):
    return [(p * PAIR + y, q * PAIR + y) for p, q in links for y in range(PAIR)]


def move(value, axes, links):
    return lax.ppermute(value, axes, links)


def grid_gather(chunk, length, pair_first):
    f = lax.axis_index("fs")
    z, y = f // PAIR, f % PAIR
    rows = chunk.shape[0]
    if length != 4:
        whole = lax.all_gather(chunk, "fs", axis=0, tiled=True)
        cut = [(i // PAIR, i % PAIR, whole[i * rows : (i + 1) * rows]) for i in range(length * PAIR)]
        middle = len(cut) // 2
        return cut[:middle], cut[middle:]

    def swap(value):
        return move(value, "fs", [(i, i ^ 1) for i in range(length * PAIR)])

    def line(first):
        got = move(first, "fs", line_pairs([(0, 1), (1, 0), (2, 3), (3, 2)]))
        near = lax.optimization_barrier(jnp.concatenate([first, got], axis=0))
        inner = move(near, "fs", line_pairs([(1, 2), (2, 1)]))
        outer = move(inner, "fs", line_pairs([(1, 0), (2, 3)]))
        return near, lax.optimization_barrier(jnp.where((z == 1) | (z == 2), inner, outer))

    mate = z ^ 1
    far_one, far_two = jnp.where(z < 2, 2, 1), jnp.where(z < 2, 3, 0)
    if pair_first:
        both = lax.optimization_barrier(jnp.concatenate([chunk, swap(chunk)], axis=0))
        near, far = line(both)
        places = [(z, y), (z, 1 - y), (mate, y), (mate, 1 - y)]
        far_places = [(far_one, y), (far_one, 1 - y), (far_two, y), (far_two, 1 - y)]
        return (
            [(*places[i], near[i * rows : (i + 1) * rows]) for i in range(4)],
            [(*far_places[i], far[i * rows : (i + 1) * rows]) for i in range(4)],
        )
    near, far = line(chunk)
    near_other, far_other = swap(near), swap(far)
    return (
        [(z, y, near[:rows]), (mate, y, near[rows:]), (z, 1 - y, near_other[:rows]), (mate, 1 - y, near_other[rows:])],
        [
            (far_one, y, far[:rows]),
            (far_two, y, far[rows:]),
            (far_one, 1 - y, far_other[:rows]),
            (far_two, 1 - y, far_other[rows:]),
        ],
    )


def body(prompt_tokens, up_master, down_master, norm_gain):
    shards = lax.axis_size("fs")
    length = shards // PAIR
    g = lax.axis_index("gr")
    t = lax.axis_index("tp")
    rows, half = up_master.shape
    width = half // lax.axis_size("tp")
    straight = t == g

    def piece(matrix, gain, u):
        cut = lax.dynamic_slice_in_dim(matrix, u * width, width, 1)
        if gain is not None:
            cut = gain[:, None] * cut
        return cut.astype(jnp.bfloat16)

    up_same, up_cross = piece(up_master, norm_gain, t), piece(up_master, norm_gain, 1 - t)
    down_same, down_cross = piece(down_master, None, t), piece(down_master, None, 1 - t)
    across = move(jnp.concatenate([up_cross, down_cross], axis=0), GROUP, [(0, 1), (3, 2)])
    up_a = lax.optimization_barrier(jnp.where(straight, up_same, across[:rows]))
    down_a = lax.optimization_barrier(jnp.where(straight, down_same, across[rows:]))

    def from_other_group(same, cross):
        near = move(same, GROUP, [(1, 3), (2, 0)])
        far = move(cross, GROUP, [(1, 2), (2, 1)])
        return lax.optimization_barrier(jnp.where(straight, near, far))

    up_b = from_other_group(up_same, up_cross)
    down_b = from_other_group(down_same, down_cross)

    values = prompt_tokens.astype(jnp.float32)
    center = jnp.mean(values, axis=-1, keepdims=True)
    variance = jnp.mean(jnp.square(values - center), axis=-1, keepdims=True)
    normed = ((values - center) * lax.rsqrt(variance + 1e-05)).astype(jnp.bfloat16)

    early = rows * 5 // 8 // 16 * 16

    def row_of(zz, yy):
        return (zz * PAIR + yy) * rows

    up_parts = [grid_gather(up_a, length, False), grid_gather(up_b, length, False)]
    down_parts = [
        (grid_gather(down_a[:-early], length, False), 0, 0),
        (grid_gather(down_b, length, False), 1, 0),
        (grid_gather(down_a[-early:], length, True), 0, rows - early),
    ]

    def base_of(cls):
        return (g if cls == 0 else 1 - g) * (shards * rows)

    total = rows * shards * lax.axis_size("gr")
    sampler_up = jnp.zeros((total, width), jnp.bfloat16)
    for cls, part in enumerate(up_parts):
        for zz, yy, block in part[0] + part[1]:
            sampler_up = lax.dynamic_update_slice_in_dim(sampler_up, block, base_of(cls) + row_of(zz, yy), 0)

    pairs = jnp.concatenate([normed, move(normed, GROUP, [(i, i ^ 1) for i in range(4)])], axis=0)
    tokens = jnp.concatenate([pairs, move(pairs, GROUP, [(i, i ^ 2) for i in range(4)])], axis=0)
    lifted = jax.nn.relu(jnp.dot(tokens, sampler_up, preferred_element_type=jnp.float32))
    hidden = (lifted * lifted).astype(jnp.bfloat16)
    count = normed.shape[0]

    def times_down(blocks):
        return lax.dot_general(
            hidden,
            jnp.concatenate(blocks, axis=0),
            (((1,), (1,)), ((), ())),
            preferred_element_type=jnp.float32,
        ).astype(jnp.bfloat16)

    sampler_down = jnp.zeros((total, width), jnp.bfloat16)
    prompt_out = jnp.zeros((count, total), jnp.bfloat16)
    for which in range(2):
        for part, cls, offset in down_parts:
            for zz, yy, block in part[which]:
                sampler_down = lax.dynamic_update_slice_in_dim(
                    sampler_down, block, base_of(cls) + row_of(zz, yy) + offset, 0
                )
        products = [
            (times_down([block for zz, yy, block in part[which]]), cls, offset, [(zz, yy) for zz, yy, b in part[which]])
            for part, cls, offset in down_parts
        ]
        slots = [(zz, yy) for zz, yy, block in down_parts[1][0][which]]
        own = []
        keep = rows - early
        order = [0, 2, 1, 3] if length == 4 else list(range(len(slots)))
        for i in range(len(slots)):
            j = order[i]
            own.append(products[0][0][:, i * keep : (i + 1) * keep])
            own.append(products[2][0][:, j * early : (j + 1) * early])
        class_a = jnp.concatenate(own, axis=1)
        class_b = products[1][0]
        partial = jnp.concatenate(
            [jnp.where(g == 0, class_a, class_b), jnp.where(g == 0, class_b, class_a)], axis=1
        )
        quarter = [partial[i * count : (i + 1) * count] for i in range(4)]
        got = move(jnp.concatenate([quarter[1], quarter[3]], axis=0), GROUP, [(i, i ^ 1) for i in range(4)]
        )
        mine = quarter[0].astype(jnp.float32) + got[:count].astype(jnp.float32)
        theirs = (quarter[2].astype(jnp.float32) + got[count:].astype(jnp.float32)).astype(jnp.bfloat16)
        rest = move(theirs, GROUP, [(i, i ^ 2) for i in range(4)])
        summed = (mine + rest.astype(jnp.float32)).astype(jnp.bfloat16)
        for side in range(2):
            for i, (zz, yy) in enumerate(slots):
                col = (side * len(slots) + i) * rows
                prompt_out = lax.dynamic_update_slice_in_dim(
                    prompt_out, summed[:, col : col + rows], side * shards * rows + row_of(zz, yy), 1
                )
    return (sampler_up, sampler_down, prompt_out)


def solution(mesh):
    placed = (
        P(("gr", "fs", "tp"), None),
        P(("gr", "fs"), "tp"),
        P(("gr", "fs"), "tp"),
        P(("gr", "fs")),
    )

    return jax.shard_map(
        body,
        mesh=mesh,
        in_specs=placed,
        out_specs=(P(None, ("gr", "tp")), P(None, ("gr", "tp")), P(("gr", "fs", "tp"), None)),
        check_vma=False,
    )
```

time: 365 us -> 341 us (0.934)
  starting transfers between devices: 0.16 us -> 49.8 us
  waiting for transfers between devices: 265 us -> 218 us
  blocking collectives: 43.9 us -> 0 us
  other arithmetic: 1.78 us -> 16.8 us
  between operations: 13.8 us -> 1.78 us
  local copies, waits for them, and re-layouts: 22.3 us -> 33.2 us
    all_gather x3 -> x0, waiting for transfers between devices: 232 us -> none  [the longest x1 116 us: body(): lax.all_gather(moved[1], 'fs', axis=0, tiled=True)]
    ppermute x0 -> x35, waiting for transfers between devices: none -> 218 us  [move(): return lax.ppermute(value, axes, links)]
    ppermute x0 -> x35, starting transfers between devices: none -> 49.8 us  [move(): return lax.ppermute(value, axes, links)]
    all_to_all x4 -> x0, blocking collectives: 43.9 us -> none  [the longest x1 18 us: body(): lax.all_to_all(lax.all_to_all(up_local, 'tp', split_axis=1, concat_axis=0...]
    reduce_scatter x1 -> x0, waiting for transfers between devices: 33 us -> none  [body(): lax.psum_scatter(lax.optimization_barrier(partial_value.astype(jnp.bfloat...]
    transpose x2 -> x0, local copies, waits for them, and re-layouts: 17.1 us -> none  [regroup(): shaped.transpose(1, 0, 2, 3)]
    dynamic_update_slice x0 -> x56, local copies, waits for them, and re-layouts: none -> 16.2 us  [the longest x24 15.1 us: body(): lax.dynamic_update_slice_in_dim(sampler_down, block, base_of(cls) + row_o...]
    convert_element_type x1 -> x5, other arithmetic: 0.11 us -> 6.01 us  [the longest x2 2.62 us: body(): summed = (mine + rest.astype(jnp.float32)).astype(jnp.bfloat16)]
  transfers between devices with their start and end apart: 4 -> 35, of which waited for: 4 -> 14; matrix products, arithmetic and copies ran while one was open for 6% -> 18% of each run, Pallas kernels for 0% -> 0%
where the time goes in v1:
time: 341 us; the launch traced here: 339 us
  waiting for transfers between devices  218 us (64%)
  starting transfers between devices  49.8 us (15%)
  local copies, waits for them, and re-layouts  33.2 us (10%)
  matrix products  19.8 us (6%)
  other arithmetic  16.8 us (5%)
    ppermute x35, waiting for transfers between devices, move(): return lax.ppermute(value, axes, links)  218 us
    ppermute x35, starting transfers between devices, move(): return lax.ppermute(value, axes, links)  49.8 us
    dynamic_update_slice x24, local copies, waits for them, and re-layouts, body(): lax.dynamic_update_slice_in_dim(sampler_down, block, base_of(cls) + row_o...  15.1 us
    dot_general x6, matrix products, times_down(): lax.dot_general(hidden, jnp.concatenate(blocks, axis=0), (((1,), (1,)), (...  12.7 us
    dot_general x1, matrix products, body(): jnp.dot(tokens, sampler_up, preferred_element_type=jnp.float32)  7.14 us
  transfers between devices with their start and end apart: 35, of which 14 were waited for; matrix products, arithmetic and copies ran while one was open for 18% of the time, Pallas kernels for 0%

profile of v1, /device:TPU:0, one launch (start us, length us, event | category | flops | bytes accessed | tf_op | source)
XLA Modules:
  0.0 339.3 jit_solution(9433910183190009543)
XLA Ops:
  0.7 1.3 dynamic-slice_convert_fusion.1
  2.0 1.4 multiply_convert_fusion.1
  4.4 3.4 collective-permute-start
  9.4 1.5 collective-permute-start.16
  10.9 3.0 slice_select_fusion
  14.0 2.5 collective-permute-start.13
  16.4 1.1 pad_maximum_fusion.1
  17.7 1.3 collective-permute-start.6
  20.1 2.0 collective-permute-start.19
  23.2 3.9 %collective-permute-done.19 = bf16[80,2048]{1,0:T(8,128)(2,1)S(1)} collective-permute-done((bf16[80,2048]{1,0:T(8,128)(2,1)S(1)}, bf16[80,2048]{1,0:T(8,128)(2,1)S(1)}, u32[]{:S(2)}, u32[]{:S(2)}) %collective-permute-start.19) | collective-permute-done | bytes 327712 | tf_op jit(solution)/shard_map/ppermute | solution.py:16
  27.2 1.3 collective-permute-start.15
  28.5 2.0 collective-permute-start.14
  30.6 1.8 collective-permute-done.6
  32.4 1.4 collective-permute-start.21
  33.8 3.7 %collective-permute-start.20 = (bf16[160,2048]{1,0:T(8,128)(2,1)S(1)}, bf16[160,2048]{1,0:T(8,128)(2,1)S(1)}, u32[]{:S(2)}, u32[]{:S(2)}) collective-permute-start(bf16[160,2048]{1,0:T(8,128)(2,1)S(1)} %pad_maximum_fusion.8), channel_id=1, source_target_pairs={{0,4},{2,6},{4,0},{6,2},{8,12},{10,14},{12,8},{14,10},{1,5},{3,7},... | collective-permute-start | bytes 1966088 | tf_op jit(solution)/shard_map/ppermute | solution.py:16
  38.8 1.6 collective-permute-start.2
  40.4 7.2 %collective-permute-done.15 = bf16[128,2048]{1,0:T(8,128)(2,1)} collective-permute-done((bf16[128,2048]{1,0:T(8,128)(2,1)}, bf16[128,2048]{1,0:T(8,128)(2,1)}, u32[]{:S(2)}, u32[]{:S(2)}) %collective-permute-start.15) | collective-permute-done | bytes 524320 | tf_op jit(solution)/shard_map/ppermute | solution.py:16
  48.4 1.1 broadcast_select_fusion.8
  49.6 4.4 %collective-permute-start.8 = (bf16[128,2048]{1,0:T(8,128)(2,1)S(1)}, bf16[128,2048]{1,0:T(8,128)(2,1)S(1)}, u32[]{:S(2)}, u32[]{:S(2)}) collective-permute-start(bf16[128,2048]{1,0:T(8,128)(2,1)S(1)} %broadcast_select_fusion.9), channel_id=1, source_target_pairs={{0,4},{2,6},{4,0},{6,2},{8,12},{10,14},{12,8},{14,10},{1,5},{3,7},... | collective-permute-start | bytes 1572872 | tf_op jit(solution)/shard_map/ppermute | solution.py:16
  54.0 1.3 collective-permute-start.22
  57.2 15.7 %collective-permute-done.22 = bf16[96,2048]{1,0:T(8,128)(2,1)S(1)} collective-permute-done((bf16[96,2048]{1,0:T(8,128)(2,1)}, bf16[96,2048]{1,0:T(8,128)(2,1)S(1)}, u32[]{:S(2)}, u32[]{:S(2)}) %collective-permute-start.22) | collective-permute-done | bytes 393248 | tf_op jit(solution)/shard_map/ppermute | solution.py:16
  72.9 1.6 collective-permute-start.23
  74.6 9.9 %collective-permute-done.17 = bf16[128,2048]{1,0:T(8,128)(2,1)S(1)} collective-permute-done((bf16[128,2048]{1,0:T(8,128)(2,1)S(1)}, bf16[128,2048]{1,0:T(8,128)(2,1)S(1)}, u32[]{:S(2)}, u32[]{:S(2)}) %collective-permute-start.17) | collective-permute-done | bytes 524320 | tf_op jit(solution)/shard_map/ppermute | solution.py:16
  85.4 1.6 collective-permute-start.18
  88.7 18.8 %collective-permute-done.18 = bf16[256,2048]{1,0:T(8,128)(2,1)S(1)} collective-permute-done((bf16[256,2048]{1,0:T(8,128)(2,1)S(1)}, bf16[256,2048]{1,0:T(8,128)(2,1)S(1)}, u32[]{:S(2)}, u32[]{:S(2)}) %collective-permute-start.18) | collective-permute-done | bytes 1048608 | tf_op jit(solution)/shard_map/ppermute | solution.py:16
  107.5 1.3 collective-permute-start.4
  109.1 5.5 %collective-permute-start.30 = (bf16[288,2048]{1,0:T(8,128)(2,1)S(1)}, bf16[288,2048]{1,0:T(8,128)(2,1)S(1)}, u32[]{:S(2)}, u32[]{:S(2)}) collective-permute-start(bf16[288,2048]{1,0:T(8,128)(2,1)S(1)} %copy-done.7), channel_id=1, source_target_pairs={{0,16},{1,17},{16,0},{17,1},{2,18},{3,19},{18,2},{19,3},{4,20},{5,... | collective-permute-start | bytes 3538952 | tf_op jit(solution)/shard_map/ppermute | solution.py:16
  115.7 1.3 collective-permute-start.11
  117.0 1.3 collective-permute-start.25
  118.3 14.1 %collective-permute-done.4 = bf16[256,2048]{1,0:T(8,128)(2,1)S(1)} collective-permute-done((bf16[256,2048]{1,0:T(8,128)(2,1)S(1)}, bf16[256,2048]{1,0:T(8,128)(2,1)S(1)}, u32[]{:S(2)}, u32[]{:S(2)}) %collective-permute-start.4) | collective-permute-done | bytes 1048608 | tf_op jit(solution)/shard_map/ppermute | solution.py:16
  132.4 1.3 collective-permute-start.28
  134.0 75.3 %collective-permute-done.25 = bf16[256,2048]{1,0:T(8,128)(2,1)S(1)} collective-permute-done((bf16[256,2048]{1,0:T(8,128)(2,1)S(1)}, bf16[256,2048]{1,0:T(8,128)(2,1)S(1)}, u32[]{:S(2)}, u32[]{:S(2)}) %collective-permute-start.25) | collective-permute-done | bytes 1048608 | tf_op jit(solution)/shard_map/ppermute | solution.py:16
  209.7 1.1 broadcast_select_fusion.1
  210.8 1.5 collective-permute-start.26
  212.5 1.1 slice_dynamic-update-slice_fusion.3
  213.6 1.1 slice_dynamic-update-slice_fusion.2
  214.7 18.5 %collective-permute-done.28 = bf16[320,2048]{1,0:T(8,128)(2,1)S(1)} collective-permute-done((bf16[320,2048]{1,0:T(8,128)(2,1)S(1)}, bf16[320,2048]{1,0:T(8,128)(2,1)S(1)}, u32[]{:S(2)}, u32[]{:S(2)}) %collective-permute-start.28) | collective-permute-done | bytes 1310752 | tf_op jit(solution)/shard_map/ppermute | solution.py:16
  233.9 1.4 collective-permute-done.5
  235.7 35.4 %collective-permute-done.12 = bf16[256,2048]{1,0:T(8,128)(2,1)S(1)} collective-permute-done((bf16[256,2048]{1,0:T(8,128)(2,1)S(1)}, bf16[256,2048]{1,0:T(8,128)(2,1)S(1)}, u32[]{:S(2)}, u32[]{:S(2)}) %collective-permute-start.12) | collective-permute-done | bytes 1048608 | tf_op jit(solution)/shard_map/ppermute | solution.py:16
  271.3 7.1 %multiply_convert_fusion = bf16[576,2048]{1,0:T(8,128)(2,1)S(1)} fusion(bf16[2048,2048]{1,0:T(8,128)(2,1)S(1)} %slice_dynamic-update-slice_fusion.8, bf16[288,2048]{1,0:T(8,128)(2,1)S(1)} %collective-permute-done.30, bf16[144,2048]{1,0:T(8,128)(2,1)S(1)} %copy-done.10, bf16[144,2048]{1,0:T(8,128)(2,1)S(1)} %fusion.22), kind=kOutput, calls=%fused_computation | convolution fusion | flops 4842455040 | bytes 13107200 | tf_op jit(solution)/shard_map/dot_general | solution.py:120
  278.5 1.2 convolution_convert_fusion.1
  279.7 2.0 convolution_convert_fusion.3
  281.9 1.8 broadcast_select_fusion.6
  284.5 1.1 copy.26
  285.6 3.0 convolution_convert_fusion.2
  288.6 1.2 convolution_convert_fusion
  290.0 3.4 broadcast_select_fusion.4
  294.2 1.1 copy.38
  295.6 1.9 slice_dynamic-update-slice_fusion.1
  297.5 1.9 slice_dynamic-update-slice_fusion
  299.4 1.7 slice_dynamic-update-slice_fusion.27
  301.1 1.7 slice_dynamic-update-slice_fusion.26
  302.8 1.7 slice_dynamic-update-slice_fusion.25
  304.6 1.7 slice_dynamic-update-slice_fusion.24
  306.3 1.8 fusion.41
  308.1 1.2 copy.52
  310.3 1.9 fusion.40
  313.2 1.2 copy.54
  315.4 2.0 collective-permute-start.34
  317.4 1.2 copy.53
  318.6 6.8 %collective-permute-done.32 = bf16[144,1024]{0,1:T(8,128)(2,1)} collective-permute-done((bf16[144,1024]{0,1:T(8,128)(2,1)}, bf16[144,1024]{0,1:T(8,128)(2,1)}, u32[]{:S(2)}, u32[]{:S(2)}) %collective-permute-start.32) | collective-permute-done | bytes 294944 | tf_op jit(solution)/shard_map/ppermute | solution.py:16
  325.4 1.4 add_convert_fusion.2
  327.8 8.0 %collective-permute-done.34 = bf16[144,1024]{0,1:T(8,128)(2,1)} collective-permute-done((bf16[144,1024]{0,1:T(8,128)(2,1)}, bf16[144,1024]{0,1:T(8,128)(2,1)}, u32[]{:S(2)}, u32[]{:S(2)}) %collective-permute-start.34) | collective-permute-done | bytes 294944 | tf_op jit(solution)/shard_map/ppermute | solution.py:16
  335.8 1.2 add_convert_fusion
  (179 shorter events, 23.4 us)
Async XLA Ops:
  0.6 10.3 %copy-start.13 = (f32[128]{0:T(128)S(1)}, f32[128]{0:T(128)}, u32[]{:S(2)}) copy-start(f32[128]{0:T(128)} %param.7) | copy-start | bytes 1540
  0.6 7.2 %copy-start.2 = (bf16[144,2048]{1,0:T(8,128)(2,1)S(1)}, bf16[144,2048]{1,0:T(8,128)(2,1)}, u32[]{:S(2)}) copy-start(bf16[144,2048]{1,0:T(8,128)(2,1)} %param.4) | copy-start | bytes 1769476
  4.4 6.5 %collective-permute-start = (bf16[256,2048]{1,0:T(8,128)(2,1)}, bf16[256,2048]{1,0:T(8,128)(2,1)}, u32[]{:S(2)}, u32[]{:S(2)}) collective-permute-start(bf16[256,2048]{1,0:T(8,128)(2,1)} %pad_maximum_fusion.2), channel_id=1, source_target_pairs={{0,1},{17,16},{2,3},{19,18},{4,5},{21,20},{6,7},{23,22},{8,9},{25,... | collective-permute-start | bytes 3145736 | tf_op jit(solution)/shard_map/ppermute | solution.py:16
  8.7 7.8 %collective-permute-start.29 = (bf16[144,2048]{1,0:T(8,128)(2,1)S(1)}, bf16[144,2048]{1,0:T(8,128)(2,1)S(1)}, u32[]{:S(2)}, u32[]{:S(2)}) collective-permute-start(bf16[144,2048]{1,0:T(8,128)(2,1)S(1)} %fusion.22), channel_id=1, source_target_pairs={{0,1},{1,0},{16,17},{17,16},{2,3},{3,2},{18,19},{19,18},{4,5},{5,4... | collective-permute-start | bytes 1769480 | tf_op jit(solution)/shard_map/ppermute | solution.py:16
  8.7 19.8 %collective-permute-start.7 = (bf16[128,2048]{1,0:T(8,128)(2,1)S(1)}, bf16[128,2048]{1,0:T(8,128)(2,1)S(1)}, u32[]{:S(2)}, u32[]{:S(2)}) collective-permute-start(bf16[128,2048]{1,0:T(8,128)(2,1)S(1)} %multiply_convert_fusion.1), channel_id=1, source_target_pairs={{1,16},{16,1},{3,18},{18,3},{5,20},{20,5},{7,22},{22,7},{9,24},{24... | collective-permute-start | bytes 1572872 | tf_op jit(solution)/shard_map/ppermute | solution.py:16
  9.4 29.4 %collective-permute-start.16 = (bf16[128,2048]{1,0:T(8,128)(2,1)S(1)}, bf16[128,2048]{1,0:T(8,128)(2,1)}, u32[]{:S(2)}, u32[]{:S(2)}) collective-permute-start(bf16[128,2048]{1,0:T(8,128)(2,1)S(1)} %dynamic-slice_convert_fusion.1), channel_id=1, source_target_pairs={{1,16},{16,1},{3,18},{18,3},{5,20},{20,5},{7,22},{22,7},{9,24},{24... | collective-permute-start | bytes 1572872 | tf_op jit(solution)/shard_map/ppermute | solution.py:16
  14.0 6.1 %collective-permute-start.13 = (bf16[48,2048]{1,0:T(8,128)(2,1)S(1)}, bf16[48,2048]{1,0:T(8,128)(2,1)S(1)}, u32[]{:S(2)}, u32[]{:S(2)}) collective-permute-start(bf16[48,2048]{1,0:T(8,128)(2,1)S(1)} %slice.380), channel_id=1, source_target_pairs={{0,4},{2,6},{4,0},{6,2},{8,12},{10,14},{12,8},{14,10},{1,5},{3,7},... | collective-permute-start | bytes 589832 | tf_op jit(solution)/shard_map/ppermute | solution.py:16
  16.4 6.7 %copy-start.9 = (bf16[144,2048]{1,0:T(8,128)(2,1)}, bf16[144,2048]{1,0:T(8,128)(2,1)S(1)}, u32[]{:S(2)}) copy-start(bf16[144,2048]{1,0:T(8,128)(2,1)S(1)} %collective-permute-done.29) | copy-start | bytes 1769476
  17.6 16.2 %collective-permute-start.1 = (bf16[128,2048]{1,0:T(8,128)(2,1)S(1)}, bf16[128,2048]{1,0:T(8,128)(2,1)S(1)}, u32[]{:S(2)}, u32[]{:S(2)}) collective-permute-start(bf16[128,2048]{1,0:T(8,128)(2,1)S(1)} %get-tuple-element.15), channel_id=1, source_target_pairs={{0,4},{2,6},{4,0},{6,2},{8,12},{10,14},{12,8},{14,10},{1,5},{3,7},... | collective-permute-start | bytes 1572872 | tf_op jit(solution)/shard_map/ppermute | solution.py:16
  17.7 14.6 %collective-permute-start.6 = (bf16[128,2048]{1,0:T(8,128)(2,1)S(1)}, bf16[128,2048]{1,0:T(8,128)(2,1)S(1)}, u32[]{:S(2)}, u32[]{:S(2)}) collective-permute-start(bf16[128,2048]{1,0:T(8,128)(2,1)S(1)} %get-tuple-element.16), channel_id=1, source_target_pairs={{1,17},{16,0},{3,19},{18,2},{5,21},{20,4},{7,23},{22,6},{9,25},{24... | collective-permute-start | bytes 1572872 | tf_op jit(solution)/shard_map/ppermute | solution.py:16
  20.1 7.1 %collective-permute-start.19 = (bf16[80,2048]{1,0:T(8,128)(2,1)S(1)}, bf16[80,2048]{1,0:T(8,128)(2,1)S(1)}, u32[]{:S(2)}, u32[]{:S(2)}) collective-permute-start(bf16[80,2048]{1,0:T(8,128)(2,1)S(1)} %slice.389), channel_id=1, source_target_pairs={{0,2},{2,0},{4,6},{6,4},{8,10},{10,8},{12,14},{14,12},{1,3},{3,1},... | collective-permute-start | bytes 983048 | tf_op jit(solution)/shard_map/ppermute | solution.py:16
  22.1 10.3 %copy-start.4 = (bf16[96,2048]{1,0:T(8,128)(2,1)}, bf16[96,2048]{1,0:T(8,128)(2,1)S(1)}, u32[]{:S(2)}) copy-start(bf16[96,2048]{1,0:T(8,128)(2,1)S(1)} %pad_maximum_fusion.11) | copy-start | bytes 1179652
  27.2 20.5 %collective-permute-start.15 = (bf16[128,2048]{1,0:T(8,128)(2,1)}, bf16[128,2048]{1,0:T(8,128)(2,1)}, u32[]{:S(2)}, u32[]{:S(2)}) collective-permute-start(bf16[128,2048]{1,0:T(8,128)(2,1)} %get-tuple-element.4), channel_id=1, source_target_pairs={{1,17},{16,0},{3,19},{18,2},{5,21},{20,4},{7,23},{22,6},{9,25},{24... | collective-permute-start | bytes 1572872 | tf_op jit(solution)/shard_map/ppermute | solution.py:16
  28.5 3.8 %copy-start.11 = (bf16[128,2048]{1,0:T(8,128)(2,1)}, bf16[128,2048]{1,0:T(8,128)(2,1)S(1)}, u32[]{:S(2)}) copy-start(bf16[128,2048]{1,0:T(8,128)(2,1)S(1)} %collective-permute-done.7) | copy-start | bytes 1572868
  28.5 21.0 %collective-permute-start.14 = (bf16[96,2048]{1,0:T(8,128)(2,1)S(1)}, bf16[96,2048]{1,0:T(8,128)(2,1)}, u32[]{:S(2)}, u32[]{:S(2)}) collective-permute-start(bf16[96,2048]{1,0:T(8,128)(2,1)S(1)} %pad_maximum_fusion.11), channel_id=1, source_target_pairs={{0,2},{2,0},{4,6},{6,4},{8,10},{10,8},{12,14},{14,12},{1,3},{3,1},... | collective-permute-start | bytes 1179656 | tf_op jit(solution)/shard_map/ppermute | solution.py:16
  32.4 21.6 %collective-permute-start.21 = (bf16[96,2048]{1,0:T(8,128)(2,1)S(1)}, bf16[96,2048]{1,0:T(8,128)(2,1)}, u32[]{:S(2)}, u32[]{:S(2)}) collective-permute-start(bf16[96,2048]{1,0:T(8,128)(2,1)S(1)} %pad_maximum_fusion.11), channel_id=1, source_target_pairs={{4,8},{6,10},{8,4},{10,6},{5,9},{7,11},{9,5},{11,7},{20,24},{22,26... | collective-permute-start | bytes 1179656 | tf_op jit(solution)/shard_map/ppermute | solution.py:16
  33.8 39.0 %collective-permute-start.20 = (bf16[160,2048]{1,0:T(8,128)(2,1)S(1)}, bf16[160,2048]{1,0:T(8,128)(2,1)S(1)}, u32[]{:S(2)}, u32[]{:S(2)}) collective-permute-start(bf16[160,2048]{1,0:T(8,128)(2,1)S(1)} %pad_maximum_fusion.8), channel_id=1, source_target_pairs={{0,4},{2,6},{4,0},{6,2},{8,12},{10,14},{12,8},{14,10},{1,5},{3,7},... | collective-permute-start | bytes 1966088 | tf_op jit(solution)/shard_map/ppermute | solution.py:16
  38.8 48.3 %collective-permute-start.2 = (bf16[256,2048]{1,0:T(8,128)(2,1)S(1)}, bf16[256,2048]{1,0:T(8,128)(2,1)S(1)}, u32[]{:S(2)}, u32[]{:S(2)}) collective-permute-start(bf16[256,2048]{1,0:T(8,128)(2,1)S(1)} %pad_maximum_fusion.3), channel_id=1, source_target_pairs={{0,2},{2,0},{4,6},{6,4},{8,10},{10,8},{12,14},{14,12},{1,3},{3,1},... | collective-permute-start | bytes 3145736 | tf_op jit(solution)/shard_map/ppermute | solution.py:16
  47.7 40.3 %collective-permute-start.3 = (bf16[256,2048]{1,0:T(8,128)(2,1)S(1)}, bf16[256,2048]{1,0:T(8,128)(2,1)S(1)}, u32[]{:S(2)}, u32[]{:S(2)}) collective-permute-start(bf16[256,2048]{1,0:T(8,128)(2,1)S(1)} %pad_maximum_fusion.3), channel_id=1, source_target_pairs={{4,8},{6,10},{8,4},{10,6},{5,9},{7,11},{9,5},{11,7},{20,24},{22,26... | collective-permute-start | bytes 3145736 | tf_op jit(solution)/shard_map/ppermute | solution.py:16
  49.6 35.9 %collective-permute-start.8 = (bf16[128,2048]{1,0:T(8,128)(2,1)S(1)}, bf16[128,2048]{1,0:T(8,128)(2,1)S(1)}, u32[]{:S(2)}, u32[]{:S(2)}) collective-permute-start(bf16[128,2048]{1,0:T(8,128)(2,1)S(1)} %broadcast_select_fusion.9), channel_id=1, source_target_pairs={{0,4},{2,6},{4,0},{6,2},{8,12},{10,14},{12,8},{14,10},{1,5},{3,7},... | collective-permute-start | bytes 1572872 | tf_op jit(solution)/shard_map/ppermute | solution.py:16
  54.0 18.9 %collective-permute-start.22 = (bf16[96,2048]{1,0:T(8,128)(2,1)}, bf16[96,2048]{1,0:T(8,128)(2,1)S(1)}, u32[]{:S(2)}, u32[]{:S(2)}) collective-permute-start(bf16[96,2048]{1,0:T(8,128)(2,1)} %collective-permute-done.21), channel_id=1, source_target_pairs={{4,0},{6,2},{8,12},{10,14},{5,1},{7,3},{9,13},{11,15},{20,16},{22,... | collective-permute-start | bytes 1179656 | tf_op jit(solution)/shard_map/ppermute | solution.py:16
  72.8 11.6 %collective-permute-start.17 = (bf16[128,2048]{1,0:T(8,128)(2,1)S(1)}, bf16[128,2048]{1,0:T(8,128)(2,1)S(1)}, u32[]{:S(2)}, u32[]{:S(2)}) collective-permute-start(bf16[128,2048]{1,0:T(8,128)(2,1)S(1)} %broadcast_select_fusion.8), channel_id=1, source_target_pairs={{0,4},{2,6},{4,0},{6,2},{8,12},{10,14},{12,8},{14,10},{1,5},{3,7},... | collective-permute-start | bytes 1572872 | tf_op jit(solution)/shard_map/ppermute | solution.py:16
  72.9 36.2 %copy-start.6 = (bf16[96,2048]{1,0:T(8,128)(2,1)}, bf16[96,2048]{1,0:T(8,128)(2,1)S(1)}, u32[]{:S(2)}) copy-start(bf16[96,2048]{1,0:T(8,128)(2,1)S(1)} %broadcast_select_fusion.10) | copy-start | bytes 1179652
  72.9 36.2 %collective-permute-start.23 = (bf16[96,2048]{1,0:T(8,128)(2,1)S(1)}, bf16[96,2048]{1,0:T(8,128)(2,1)S(1)}, u32[]{:S(2)}, u32[]{:S(2)}) collective-permute-start(bf16[96,2048]{1,0:T(8,128)(2,1)S(1)} %broadcast_select_fusion.10), channel_id=1, source_target_pairs={{0,2},{2,0},{4,6},{6,4},{8,10},{10,8},{12,14},{14,12},{1,3},{3,1},... | collective-permute-start | bytes 1179656 | tf_op jit(solution)/shard_map/ppermute | solution.py:16
  84.4 32.6 %collective-permute-start.27 = (bf16[320,2048]{1,0:T(8,128)(2,1)S(1)}, bf16[320,2048]{1,0:T(8,128)(2,1)S(1)}, u32[]{:S(2)}, u32[]{:S(2)}) collective-permute-start(bf16[320,2048]{1,0:T(8,128)(2,1)S(1)} %pad_maximum_fusion), channel_id=1, source_target_pairs={{4,8},{6,10},{8,4},{10,6},{5,9},{7,11},{9,5},{11,7},{20,24},{22,26... | collective-permute-start | bytes 3932168 | tf_op jit(solution)/shard_map/ppermute | solution.py:16
  85.4 23.7 %copy-start.7 = (bf16[288,2048]{1,0:T(8,128)(2,1)S(1)}, bf16[288,2048]{1,0:T(8,128)(2,1)}, u32[]{:S(2)}) copy-start(bf16[288,2048]{1,0:T(8,128)(2,1)} %pad_maximum_fusion.1) | copy-start | bytes 3538948
  85.4 22.1 %collective-permute-start.18 = (bf16[256,2048]{1,0:T(8,128)(2,1)S(1)}, bf16[256,2048]{1,0:T(8,128)(2,1)S(1)}, u32[]{:S(2)}, u32[]{:S(2)}) collective-permute-start(bf16[256,2048]{1,0:T(8,128)(2,1)S(1)} %pad_maximum_fusion.5), channel_id=1, source_target_pairs={{0,2},{2,0},{4,6},{6,4},{8,10},{10,8},{12,14},{14,12},{1,3},{3,1},... | collective-permute-start | bytes 3145736 | tf_op jit(solution)/shard_map/ppermute | solution.py:16
  87.1 28.6 %collective-permute-start.24 = (bf16[256,2048]{1,0:T(8,128)(2,1)S(1)}, bf16[256,2048]{1,0:T(8,128)(2,1)S(1)}, u32[]{:S(2)}, u32[]{:S(2)}) collective-permute-start(bf16[256,2048]{1,0:T(8,128)(2,1)S(1)} %pad_maximum_fusion.5), channel_id=1, source_target_pairs={{4,8},{6,10},{8,4},{10,6},{5,9},{7,11},{9,5},{11,7},{20,24},{22,26... | collective-permute-start | bytes 3145736 | tf_op jit(solution)/shard_map/ppermute | solution.py:16
  88.0 26.7 %collective-permute-start.10 = (bf16[256,2048]{1,0:T(8,128)(2,1)S(1)}, bf16[256,2048]{1,0:T(8,128)(2,1)S(1)}, u32[]{:S(2)}, u32[]{:S(2)}) collective-permute-start(bf16[256,2048]{1,0:T(8,128)(2,1)S(1)} %pad_maximum_fusion.4), channel_id=1, source_target_pairs={{4,8},{6,10},{8,4},{10,6},{5,9},{7,11},{9,5},{11,7},{20,24},{22,26... | collective-permute-start | bytes 3145736 | tf_op jit(solution)/shard_map/ppermute | solution.py:16
  107.5 25.0 %collective-permute-start.4 = (bf16[256,2048]{1,0:T(8,128)(2,1)S(1)}, bf16[256,2048]{1,0:T(8,128)(2,1)S(1)}, u32[]{:S(2)}, u32[]{:S(2)}) collective-permute-start(bf16[256,2048]{1,0:T(8,128)(2,1)S(1)} %collective-permute-done.3), channel_id=1, source_target_pairs={{4,0},{6,2},{8,12},{10,14},{5,1},{7,3},{9,13},{11,15},{20,16},{22,... | collective-permute-start | bytes 3145736 | tf_op jit(solution)/shard_map/ppermute | solution.py:16
  109.1 23.3 %copy-start.12 = (bf16[96,2048]{1,0:T(8,128)(2,1)}, bf16[96,2048]{1,0:T(8,128)(2,1)S(1)}, u32[]{:S(2)}) copy-start(bf16[96,2048]{1,0:T(8,128)(2,1)S(1)} %collective-permute-done.23) | copy-start | bytes 1179652
  109.1 162.1 %collective-permute-start.30 = (bf16[288,2048]{1,0:T(8,128)(2,1)S(1)}, bf16[288,2048]{1,0:T(8,128)(2,1)S(1)}, u32[]{:S(2)}, u32[]{:S(2)}) collective-permute-start(bf16[288,2048]{1,0:T(8,128)(2,1)S(1)} %copy-done.7), channel_id=1, source_target_pairs={{0,16},{1,17},{16,0},{17,1},{2,18},{3,19},{18,2},{19,3},{4,20},{5,... | collective-permute-start | bytes 3538952 | tf_op jit(solution)/shard_map/ppermute | solution.py:16
  114.7 120.8 %collective-permute-start.9 = (bf16[256,2048]{1,0:T(8,128)(2,1)S(1)}, bf16[256,2048]{1,0:T(8,128)(2,1)S(1)}, u32[]{:S(2)}, u32[]{:S(2)}) collective-permute-start(bf16[256,2048]{1,0:T(8,128)(2,1)S(1)} %pad_maximum_fusion.4), channel_id=1, source_target_pairs={{0,2},{2,0},{4,6},{6,4},{8,10},{10,8},{12,14},{14,12},{1,3},{3,1},... | collective-permute-start | bytes 3145736 | tf_op jit(solution)/shard_map/ppermute | solution.py:16
  115.7 95.1 %collective-permute-start.11 = (bf16[256,2048]{1,0:T(8,128)(2,1)S(1)}, bf16[256,2048]{1,0:T(8,128)(2,1)S(1)}, u32[]{:S(2)}, u32[]{:S(2)}) collective-permute-start(bf16[256,2048]{1,0:T(8,128)(2,1)S(1)} %collective-permute-done.10), channel_id=1, source_target_pairs={{4,0},{6,2},{8,12},{10,14},{5,1},{7,3},{9,13},{11,15},{20,16},{22,... | collective-permute-start | bytes 3145736 | tf_op jit(solution)/shard_map/ppermute | solution.py:16
  117.0 92.2 %collective-permute-start.25 = (bf16[256,2048]{1,0:T(8,128)(2,1)S(1)}, bf16[256,2048]{1,0:T(8,128)(2,1)S(1)}, u32[]{:S(2)}, u32[]{:S(2)}) collective-permute-start(bf16[256,2048]{1,0:T(8,128)(2,1)S(1)} %collective-permute-done.24), channel_id=1, source_target_pairs={{4,0},{6,2},{8,12},{10,14},{5,1},{7,3},{9,13},{11,15},{20,16},{22,... | collective-permute-start | bytes 3145736 | tf_op jit(solution)/shard_map/ppermute | solution.py:16
  132.4 100.8 %collective-permute-start.28 = (bf16[320,2048]{1,0:T(8,128)(2,1)S(1)}, bf16[320,2048]{1,0:T(8,128)(2,1)S(1)}, u32[]{:S(2)}, u32[]{:S(2)}) collective-permute-start(bf16[320,2048]{1,0:T(8,128)(2,1)S(1)} %collective-permute-done.27), channel_id=1, source_target_pairs={{4,0},{6,2},{8,12},{10,14},{5,1},{7,3},{9,13},{11,15},{20,16},{22,... | collective-permute-start | bytes 3932168 | tf_op jit(solution)/shard_map/ppermute | solution.py:16
  209.2 26.0 %collective-permute-start.5 = (bf16[256,2048]{1,0:T(8,128)(2,1)S(1)}, bf16[256,2048]{1,0:T(8,128)(2,1)S(1)}, u32[]{:S(2)}, u32[]{:S(2)}) collective-permute-start(bf16[256,2048]{1,0:T(8,128)(2,1)S(1)} %broadcast_select_fusion.3), channel_id=1, source_target_pairs={{0,2},{2,0},{4,6},{6,4},{8,10},{10,8},{12,14},{14,12},{1,3},{3,1},... | collective-permute-start | bytes 3145736 | tf_op jit(solution)/shard_map/ppermute | solution.py:16
  210.8 79.2 %collective-permute-start.26 = (bf16[256,2048]{1,0:T(8,128)(2,1)}, bf16[256,2048]{1,0:T(8,128)(2,1)}, u32[]{:S(2)}, u32[]{:S(2)}) collective-permute-start(bf16[256,2048]{1,0:T(8,128)(2,1)} %broadcast_select_fusion.1), channel_id=1, source_target_pairs={{0,2},{2,0},{4,6},{6,4},{8,10},{10,8},{12,14},{14,12},{1,3},{3,1},... | collective-permute-start | bytes 3145736 | tf_op jit(solution)/shard_map/ppermute | solution.py:16
  214.7 20.9 %copy-start.1 = (bf16[2048,2048]{1,0:T(8,128)(2,1)}, bf16[2048,2048]{1,0:T(8,128)(2,1)S(1)}, u32[]{:S(2)}) copy-start(bf16[2048,2048]{1,0:T(8,128)(2,1)S(1)} %slice_dynamic-update-slice_fusion.2) | copy-start | bytes 25165828
  233.2 37.9 %collective-permute-start.12 = (bf16[256,2048]{1,0:T(8,128)(2,1)S(1)}, bf16[256,2048]{1,0:T(8,128)(2,1)S(1)}, u32[]{:S(2)}, u32[]{:S(2)}) collective-permute-start(bf16[256,2048]{1,0:T(8,128)(2,1)S(1)} %broadcast_select_fusion.2), channel_id=1, source_target_pairs={{0,2},{2,0},{4,6},{6,4},{8,10},{10,8},{12,14},{14,12},{1,3},{3,1},... | collective-permute-start | bytes 3145736 | tf_op jit(solution)/shard_map/ppermute | solution.py:16
  233.9 54.8 %copy-start.3 = (bf16[320,2048]{1,0:T(8,128)(2,1)}, bf16[320,2048]{1,0:T(8,128)(2,1)S(1)}, u32[]{:S(2)}) copy-start(bf16[320,2048]{1,0:T(8,128)(2,1)S(1)} %broadcast_select_fusion) | copy-start | bytes 3932164
  235.3 36.0 %copy-start.10 = (bf16[144,2048]{1,0:T(8,128)(2,1)S(1)}, bf16[144,2048]{1,0:T(8,128)(2,1)}, u32[]{:S(2)}) copy-start(bf16[144,2048]{1,0:T(8,128)(2,1)} %copy-done.9) | copy-start | bytes 1769476
  271.2 7.2 %copy-start = (bf16[2048,2048]{1,0:T(8,128)(2,1)}, bf16[2048,2048]{1,0:T(8,128)(2,1)S(1)}, u32[]{:S(2)}) copy-start(bf16[2048,2048]{1,0:T(8,128)(2,1)S(1)} %slice_dynamic-update-slice_fusion.8) | copy-start | bytes 25165828
  278.4 3.5 %copy-start.14 = (bf16[576,2048]{1,0:T(8,128)(2,1)}, bf16[576,2048]{1,0:T(8,128)(2,1)S(1)}, u32[]{:S(2)}) copy-start(bf16[576,2048]{1,0:T(8,128)(2,1)S(1)} %multiply_convert_fusion) | copy-start | bytes 7077892
  278.4 1.3 copy-start.5
  285.6 3.0 copy-start.15
  285.6 20.7 %collective-permute-start.31 = (bf16[288,1024]{1,0:T(8,128)(2,1)}, bf16[288,1024]{1,0:T(8,128)(2,1)}, u32[]{:S(2)}, u32[]{:S(2)}) collective-permute-start(bf16[288,1024]{1,0:T(8,128)(2,1)} %copy.26), channel_id=1, source_target_pairs={{0,1},{1,0},{16,17},{17,16},{2,3},{3,2},{18,19},{19,18},{4,5},{5,4... | collective-permute-start | bytes 1769480 | tf_op jit(solution)/shard_map/ppermute | solution.py:16
  295.3 15.0 %collective-permute-start.33 = (bf16[288,1024]{1,0:T(8,128)(2,1)}, bf16[288,1024]{1,0:T(8,128)(2,1)}, u32[]{:S(2)}, u32[]{:S(2)}) collective-permute-start(bf16[288,1024]{1,0:T(8,128)(2,1)} %copy.38), channel_id=1, source_target_pairs={{0,1},{1,0},{16,17},{17,16},{2,3},{3,2},{18,19},{19,18},{4,5},{5,4... | collective-permute-start | bytes 1769480 | tf_op jit(solution)/shard_map/ppermute | solution.py:16
  310.3 15.1 %collective-permute-start.32 = (bf16[144,1024]{0,1:T(8,128)(2,1)}, bf16[144,1024]{0,1:T(8,128)(2,1)}, u32[]{:S(2)}, u32[]{:S(2)}) collective-permute-start(bf16[144,1024]{0,1:T(8,128)(2,1)} %add_convert_fusion.3), channel_id=1, source_target_pairs={{0,16},{1,17},{16,0},{17,1},{2,18},{3,19},{18,2},{19,3},{4,20},{5,... | collective-permute-start | bytes 884744 | tf_op jit(solution)/shard_map/ppermute | solution.py:16
  315.4 20.4 %collective-permute-start.34 = (bf16[144,1024]{0,1:T(8,128)(2,1)}, bf16[144,1024]{0,1:T(8,128)(2,1)}, u32[]{:S(2)}, u32[]{:S(2)}) collective-permute-start(bf16[144,1024]{0,1:T(8,128)(2,1)} %add_convert_fusion.1), channel_id=1, source_target_pairs={{0,16},{1,17},{16,0},{17,1},{2,18},{3,19},{18,2},{19,3},{4,20},{5,... | collective-permute-start | bytes 884744 | tf_op jit(solution)/shard_map/ppermute | solution.py:16
  338.5 0.8 copy-start.8
